TPU v7x, 256 devices: a whole 4x4x8 slice. The times are simulated.
256 devices in a mesh: ep: 16 (over y, x), tp: 16 (over z, core).
Axes of the slice: x: 4, y: 4, z: 8, core: 2. Of those that a mesh axis runs over, the one named last changes fastest.
Arguments:
- query_latent: bfloat16 [8192, 1024], P('ep'), may hold values from -6 to 6
- joint_latent: bfloat16 [8192, 512], P('ep'), may hold values from -6 to 6
- rotary_key: bfloat16 [8192, 32], P('ep'), may hold values from -60 to 60
- query_gain: float32 [1024], replicated, may hold values from 0.1 to 1.9
- joint_gain: float32 [512], replicated, may hold values from 0.1 to 1.9
- query_weight: bfloat16 [1024, 2048], P(None, 'tp'), may hold values from -0.1875 to 0.1875
- query_rotary: bfloat16 [1024, 1024], P(None, 'tp'), may hold values from -0.1875 to 0.1875
- key_weight: bfloat16 [512, 2048], P(None, 'tp'), may hold values from -0.25 to 0.25
- value_weight: bfloat16 [512, 2048], P(None, 'tp'), may hold values from -0.25 to 0.25
- output_weight: bfloat16 [2048, 2048], P('tp'), may hold values from -6 to 6
- expert_input: bfloat16 [8192, 2048], P('ep'), may hold values from -6 to 6
- expert_gain: float32 [2048], replicated, may hold values from 0.1 to 1.9
- routes: int32 [8192, 2], P('ep'), may hold values from 0 to 31, all different within a row; in each aligned block of 512 rows (0 to 511, 512 to 1023, ...) at most 48 rows name the same one
- route_weight: float32 [8192, 2], P('ep'), may hold values from 0.2 to 1
- gate_weight: bfloat16 [32, 2048, 4096], P('ep', None, 'tp'), may hold values from -0.125 to 0.125
- up_weight: bfloat16 [32, 2048, 4096], P('ep', None, 'tp'), may hold values from -0.125 to 0.125
- down_weight: bfloat16 [32, 4096, 2048], P('ep', 'tp'), may hold values from -0.09375 to 0.09375
Outputs:
- mixer_out: bfloat16 [8192, 2048], P(('ep', 'tp'))
- expert_out: bfloat16 [8192, 2048], P('ep', 'tp')
Inputs may be any that keep to these rules, and one draw needn't show every extreme that they name: `routes`: A row names 2 different experts. Among the rows of one device (aligned blocks of 512 rows) no expert is named by more than 48 rows, a bound that some block reaches.
All inputs are finite; a program needn't handle non-finite values.
Results may differ from a plain program's by a relative error of at most 0.019.
The roundings to bfloat16 on the way count: a program that leaves them out, or rounds other values in their place, can miss the bound.
Values may be sent and summed in bfloat16 or wider, within the bound.
A program may use at most 128 MiB of HBM per device.

v0:
```python
import jax
import jax.numpy as jnp
from jax import lax
from jax.sharding import PartitionSpec as P

NOPE = 64
VDIM = 64
NORM_EPSILON = 1e-06
ROTARY_BASE = 10000.0


def sent_together(arrays, axis, dim, along):
    both = jnp.concatenate(arrays, axis=along)
    out, at, outs = (lax.all_gather(both, axis, axis=dim, tiled=True), 0, [])
    for a in arrays:
        outs.append(lax.slice_in_dim(out, at, at + a.shape[along], axis=along))
        at += a.shape[along]
    return tuple(outs)


def norm_rows(source, gain_vector):
    as_float = source.astype(jnp.float32)
    factor = lax.rsqrt(jnp.mean(as_float * as_float, axis=-1, keepdims=True) + NORM_EPSILON)
    return (as_float * factor * gain_vector).astype(jnp.bfloat16)


def rotate(source, positions):
    half_width = source.shape[-1] // 2
    frequencies = ROTARY_BASE ** (-jnp.arange(half_width, dtype=jnp.float32) / half_width)
    angles = positions[:, None] * frequencies[None, :]
    view_shape = (source.shape[0],) + (1,) * (source.ndim - 2) + (half_width,)
    cosine_table = jnp.cos(angles).reshape(view_shape)
    sine_table = jnp.sin(angles).reshape(view_shape)
    first_half = source[..., :half_width]
    second = source[..., half_width:]
    return jnp.concatenate(
        [
            first_half * cosine_table - second * sine_table,
            second * cosine_table + first_half * sine_table,
        ],
        axis=-1,
    )


def attend_block(
    carried, query_plain, query_turned, key_block, value_block, turned_block, score_scale
):
    row_top, row_total, mixed_values = carried
    scores = jnp.einsum("qhd,khd->qhk", query_plain, key_block, preferred_element_type=jnp.float32)
    scores = scores + jnp.einsum(
        "qhd,kd->qhk", query_turned, turned_block, preferred_element_type=jnp.float32
    )
    scores = scores * score_scale
    new_top = jnp.maximum(row_top, jnp.max(scores, axis=-1))
    factor = jnp.exp(row_top - new_top)
    expo = jnp.exp(scores - new_top[..., None])
    row_total = row_total * factor + jnp.sum(expo, axis=-1)
    mixed_values = mixed_values * factor[..., None] + jnp.einsum(
        "qhk,khd->qhd", expo.astype(jnp.bfloat16), value_block, preferred_element_type=jnp.float32
    )
    return (new_top, row_total, mixed_values)


def token_mixer(
    query_latent,
    joint_latent,
    rotary_key,
    query_gain,
    joint_gain,
    query_weight,
    query_rotary,
    key_weight,
    value_weight,
    output_weight,
):
    row_count = query_latent.shape[0]
    head_count = key_weight.shape[1] // NOPE
    turn_width = rotary_key.shape[1]
    offset = lax.axis_index("ep") * row_count
    positions = (offset + jnp.arange(row_count, dtype=jnp.int32)).astype(jnp.float32)
    query_normed = norm_rows(query_latent, query_gain)
    joint_normed = norm_rows(joint_latent, joint_gain)
    turned_key = rotate(rotary_key.astype(jnp.float32), positions).astype(jnp.bfloat16)
    query_plain = jnp.dot(query_normed, query_weight, preferred_element_type=jnp.float32).astype(
        jnp.bfloat16
    )
    query_plain = query_plain.reshape(row_count, head_count, NOPE)
    query_turned = jnp.dot(query_normed, query_rotary, preferred_element_type=jnp.float32)
    query_turned = rotate(
        query_turned.reshape(row_count, head_count, turn_width), positions
    ).astype(jnp.bfloat16)
    score_scale = (NOPE + turn_width) ** (-0.5)
    start_carry = (
        jnp.full((row_count, head_count), -jnp.inf, jnp.float32),
        jnp.zeros((row_count, head_count), jnp.float32),
        jnp.zeros((row_count, head_count, VDIM), jnp.float32),
    )
    carried = start_carry
    latent_piece, turned_piece = sent_together((joint_normed, turned_key), "ep", 0, 1)
    block_rows = min(row_count, latent_piece.shape[0])
    block_total = latent_piece.shape[0] // block_rows

    def scan_step(inner_carry, key_items):
        latent_block, turned_block = key_items
        key_block = jnp.dot(latent_block, key_weight, preferred_element_type=jnp.float32)
        key_block = key_block.astype(jnp.bfloat16).reshape(block_rows, head_count, NOPE)
        value_block = jnp.dot(latent_block, value_weight, preferred_element_type=jnp.float32)
        value_block = value_block.astype(jnp.bfloat16).reshape(block_rows, head_count, VDIM)
        return (
            attend_block(
                inner_carry,
                query_plain,
                query_turned,
                key_block,
                value_block,
                turned_block,
                score_scale,
            ),
            None,
        )

    carried, _ = lax.scan(
        scan_step,
        carried,
        (
            latent_piece.reshape(block_total, block_rows, latent_piece.shape[1]),
            turned_piece.reshape(block_total, block_rows, turn_width),
        ),
    )
    row_top, row_total, mixed_values = carried
    attended = (
        (mixed_values / row_total[..., None])
        .astype(jnp.bfloat16)
        .reshape(row_count, head_count * VDIM)
    )
    return lax.psum_scatter(
        jnp.dot(attended, output_weight, preferred_element_type=jnp.float32).astype(jnp.bfloat16),
        "tp",
        scatter_dimension=0,
        tiled=True,
    )


def experts(expert_input, expert_gain, routes, route_weight, gate_weight, up_weight, down_weight):
    row_count = expert_input.shape[0]
    feature_width = expert_input.shape[1]
    top_count = routes.shape[1]
    group_count = lax.axis_size("ep")
    local_count = gate_weight.shape[0]
    expert_count = local_count * group_count
    capacity = 3 * row_count // (2 * group_count)
    part_width = feature_width // lax.axis_size("tp")
    flat_routes = routes.reshape(-1)
    onehot = (flat_routes[:, None] == jnp.arange(expert_count, dtype=jnp.int32)[None, :]).astype(
        jnp.int32
    )
    rank_within = jnp.sum((jnp.cumsum(onehot, axis=0) - onehot) * onehot, axis=1)
    slot_index = flat_routes * capacity + rank_within
    owner_token = jnp.arange(row_count * top_count, dtype=jnp.int32) // top_count
    slot_token = jnp.zeros((expert_count * capacity,), jnp.int32).at[slot_index].set(owner_token)
    filled = jnp.zeros((expert_count * capacity,), jnp.bfloat16).at[slot_index].set(1.0)
    normed = norm_rows(expert_input, expert_gain)
    columns = lax.dynamic_slice_in_dim(normed, lax.axis_index("tp") * part_width, part_width, 1)
    outgoing = (columns[slot_token] * filled[:, None]).reshape(
        group_count, local_count, capacity, part_width
    )
    arrived = lax.all_to_all(outgoing, "ep", split_axis=0, concat_axis=0, tiled=True)
    piece = lax.all_gather(arrived, "tp", axis=3, tiled=True)
    gate_running = jnp.einsum(
        "secd,edf->secf", piece, gate_weight, preferred_element_type=jnp.float32
    )
    up_running = jnp.einsum("secd,edf->secf", piece, up_weight, preferred_element_type=jnp.float32)
    hidden = (jax.nn.silu(gate_running) * up_running).astype(jnp.bfloat16)
    partial_value = jnp.einsum(
        "secf,efd->secd", hidden, down_weight, preferred_element_type=jnp.float32
    )
    summed = lax.psum_scatter(
        partial_value.astype(jnp.bfloat16), "tp", scatter_dimension=3, tiled=True
    )
    returned = lax.all_to_all(summed, "ep", split_axis=0, concat_axis=0, tiled=True)
    picked = returned.reshape(expert_count * capacity, part_width)[slot_index]
    picked = picked.astype(jnp.float32).reshape(row_count, top_count, part_width)
    return jnp.sum(picked * route_weight[:, :, None], axis=1).astype(jnp.bfloat16)


def local(
    query_latent,
    joint_latent,
    rotary_key,
    query_gain,
    joint_gain,
    query_weight,
    query_rotary,
    key_weight,
    value_weight,
    output_weight,
    expert_input,
    expert_gain,
    routes,
    route_weight,
    gate_weight,
    up_weight,
    down_weight,
):
    mixer_out = token_mixer(
        query_latent,
        joint_latent,
        rotary_key,
        query_gain,
        joint_gain,
        query_weight,
        query_rotary,
        key_weight,
        value_weight,
        output_weight,
    )
    expert_out = experts(
        expert_input, expert_gain, routes, route_weight, gate_weight, up_weight, down_weight
    )
    return (mixer_out, expert_out)


def solution(mesh):
    return jax.shard_map(
        local,
        mesh=mesh,
        in_specs=(
            P("ep", None),
            P("ep", None),
            P("ep", None),
            P(),
            P(),
            P(None, "tp"),
            P(None, "tp"),
            P(None, "tp"),
            P(None, "tp"),
            P("tp", None),
            P("ep", None),
            P(),
            P("ep", None),
            P("ep", None),
            P("ep", None, "tp"),
            P("ep", None, "tp"),
            P("ep", "tp", None),
        ),
        out_specs=(P(("ep", "tp"), None), P("ep", "tp")),
        check_vma=False,
    )
```

profile of v0, /device:TPU:6, one launch (start us, length us, event | category | flops | bytes accessed | tf_op | source)
XLA Modules:
  0.0 353.4 jit_solution(10818710300028206992)
XLA Ops:
  7.2 4.2 %convert_element_type.83 = f32[512,2048]{1,0:T(8,128)} convert(bf16[512,2048]{1,0:T(8,128)(2,1)} %param.29) | non-fusion elementwise | flops 1048576 | bytes 6291456 | tf_op jit(solution)/shard_map/convert_element_type | solution.py:22
  12.7 9.0 %reduce-window.6 = s32[32,8,128]{2,1,0:T(8,128)S(1)} reduce-window(s32[32,8,128]{2,1,0:T(8,128)S(1)} %fusion.46, s32[]{:T(128)} %constant.30.clone.1), window={size=1x1x128 pad=0_0x0_0x127_0}, to_apply=%region_8.9 | reduce-window | flops 4161536 | bytes 262148 | tf_op jit(solution)/shard_map/reduce-window
  22.6 4.3 %scatter_custom_fusion = s32[1536]{0:T(1024)S(1)} fusion(s32[1024]{0:T(1024)S(1)} %bitcast.150, s32[1024]{0:T(1024)S(1)} %add_select_fusion, s32[]{:T(128)} %constant.30.clone.1), kind=kCustom, calls=%fused_computation.89 | custom fusion | bytes 6148 | tf_op jit(solution)/shard_map/scatter | solution.py:160
  26.9 7.6 %scatter_custom_fusion.1 = bf16[1536]{0:T(1024)(128)(2,1)S(1)} fusion(s32[1024]{0:T(1024)S(1)} %bitcast.151, bf16[1024]{0:T(1024)(128)(2,1)S(1)} %broadcast.163, bf16[]{:T(256)} %constant.82.clone.1), kind=kCustom, calls=%fused_computation.93 | custom fusion | bytes 3074 | tf_op jit(solution)/shard_map/scatter | solution.py:161
  36.5 3.2 gather_fusion
  40.0 14.7 %all_to_all.10 = bf16[16,2,48,128]{3,2,1,0:T(8,128)(2,1)S(1)} all-to-all(bf16[16,2,48,128]{3,2,1,0:T(8,128)(2,1)S(1)} %broadcast_multiply_fusion), channel_id=1, replica_groups=mesh['ep'=16,'tp'=16] {'ep'}, dimensions={0} | all-to-all | bytes 786432 | tf_op jit(solution)/shard_map/all_to_all | solution.py:167
  57.8 1.9 pad_maximum_fusion
  60.3 1.5 fusion.38
  62.5 51.3 %all-gather.5.cloned.1.call-done = bf16[16,2,48,2048]{3,2,0,1:T(8,128)(2,1)} async-done(((bf16[16,2,48,128]{3,2,0,1:T(8,128)(2,1)}), bf16[16,2,48,2048]{3,2,0,1:T(8,128)(2,1)}) %all-gather.5.cloned.1.call-update) | async-done | bytes 6291472 | tf_op jit(solution)/shard_map/all_gather | solution.py:168
  113.8 6.3 %fusion.23 = f32[2,16,48,256]{3,2,1,0:T(8,128)} fusion(bf16[16,2,48,2048]{3,2,0,1:T(8,128)(2,1)} %all-gather.5.cloned.1.call-done, bf16[2,2048,256]{2,1,0:T(8,128)(2,1)} %param.33), kind=kOutput, calls=%fused_computation.40 | convolution fusion | flops 1610612736 | bytes 9961472 | tf_op jit(solution)/shard_map/secd,edf->secf/dot_general | solution.py:169
  120.1 10.0 %convert_bitcast_fusion = bf16[16,2,48,2048]{3,2,0,1:T(8,128)(2,1)} fusion(bf16[2,256,2048]{2,1,0:T(8,128)(2,1)S(1)} %copy-done, f32[2,16,48,256]{3,2,1,0:T(8,128)} %fusion.23, bf16[16,2,48,2048]{3,2,0,1:T(8,128)(2,1)} %all-gather.5.cloned.1.call-done, bf16[2,2048,256]{2,1,0:T(8,128)(2,1)} %param.34), kind=kOutput, calls=%fused_computation.29 | convolution fusion | flops 3226730496 | bytes 18350080 | tf_op jit(solution)/shard_map/secf,efd->secd/dot_general | solution.py:174
  130.1 23.1 %copy.56 = bf16[16,2,48,2048]{2,0,1,3:T(8,128)(2,1)} copy(bf16[16,2,48,2048]{3,2,0,1:T(8,128)(2,1)} %convert_bitcast_fusion) | data formatting | bytes 12582912
  153.2 29.8 %reshape.224 = bf16[2048,1536]{1,0:T(8,128)(2,1)} reshape(bf16[2048,2,16,48]{3,2,1,0:T(8,128)(2,1)} %bitcast.135) | data formatting | bytes 12582912
  183.3 17.5 %all-gather.3.cloned.1.call-done = bf16[8192,544]{1,0:T(8,128)(2,1)} async-done(((bf16[512,544]{1,0:T(8,128)(2,1)}), bf16[8192,544]{1,0:T(8,128)(2,1)}) %all-gather.3.cloned.1.call-update) | async-done | bytes 8912912 | tf_op jit(solution)/shard_map/all_gather | solution.py:14
  200.8 1.6 slice-done
  203.2 7.2 %slice.38 = bf16[8192,512]{1,0:T(8,128)(2,1)} slice(bf16[8192,544]{1,0:T(8,128)(2,1)} %all-gather.3.cloned.1.call-done), slice={[0:8192], [0:512]} | slice | bytes 16777216 | tf_op jit(solution)/shard_map/slice | solution.py:16
  210.4 73.0 %while.15 = (s32[]{:T(128)}, f32[512,2]{0,1:T(2,128)S(1)}, f32[512,2]{0,1:T(2,128)S(1)}, f32[512,2,64]{0,2,1:T(8,128)S(1)}, bf16[16,512,512]{2,1,0:T(8,128)(2,1)...) while((s32[]{:T(128)}, f32[512,2]{0,1:T(2,128)S(1)}, ...), condition=%wide.region_5.6_spmd.clone, body=%wide.region_2.5_spmd.clone.sunk | while | flops 305992704 | bytes 13141125 | solution.py:122
  222.2 1.4 convolution_convert_fusion.7
  228.7 1.4 convolution_convert_fusion.6
  235.9 1.4 convolution_convert_fusion.7
  240.5 1.4 convolution_convert_fusion.7
  249.6 1.4 convolution_convert_fusion.7
  263.3 1.4 convolution_convert_fusion.7
  267.9 1.4 convolution_convert_fusion.7
  283.5 3.1 convolution_convert_fusion.2
  286.7 2.1 reshape.225
  288.8 1.8 copy.48
  290.6 5.7 %all-to-all-start.1 = ((bf16[16,2,48,128]{3,2,1,0:T(8,128)(2,1)}), bf16[16,2,48,128]{3,2,1,0:T(8,128)(2,1)S(1)}, u32[]{:S(2)}, u32[]{:S(2)}) async-start(bf16[16,2,48,128]{3,2,1,0:T(8,128)(2,1)} %copy.48), calls=%async_computation.2 | async-start | bytes 786432 | tf_op jit(solution)/shard_map/all_to_all | solution.py:180
  296.5 7.1 %all-to-all-done.1 = bf16[16,2,48,128]{3,2,1,0:T(8,128)(2,1)S(1)} async-done(((bf16[16,2,48,128]{3,2,1,0:T(8,128)(2,1)}), bf16[16,2,48,128]{3,2,1,0:T(8,128)(2,1)S(1)}, u32[]{:S(2)}, u32[]{:S(2)}) %all-to-all-start.1) | async-done | bytes 393248 | tf_op jit(solution)/shard_map/all_to_all | solution.py:180
  303.6 3.2 gather_fusion.1
  306.8 3.5 fusion.37
  310.3 36.6 %reduce-scatter.5.cloned.1.call-done = bf16[32,2048]{1,0:T(8,128)(2,1)} async-done(((bf16[512,2048]{1,0:T(8,128)(2,1)}), bf16[32,2048]{1,0:T(8,128)(2,1)}) %reduce-scatter.5.cloned.1.call-update) | async-done | bytes 131088 | tf_op jit(solution)/shard_map/reduce_scatter | solution.py:136
  (226 shorter events, 72.0 us)
Async XLA Ops:
  7.2 113.0 %copy-start = (bf16[2,256,2048]{2,1,0:T(8,128)(2,1)S(1)}, bf16[2,256,2048]{2,1,0:T(8,128)(2,1)}, u32[]{:S(2)}) copy-start(bf16[2,256,2048]{2,1,0:T(8,128)(2,1)} %param.35) | copy-start | bytes 6291460
  7.2 106.6 %all-gather.5.cloned.1.call-start = ((), (), s32[]{:S(2)}) async-start(), calls=%async_computation.6 | async-start | bytes 6684672 | tf_op jit(solution)/shard_map/all_gather | solution.py:168
  7.2 4.2 %copy-start.2 = (bf16[512,2048]{1,0:T(8,128)(2,1)S(1)}, bf16[512,2048]{1,0:T(8,128)(2,1)}, u32[]{:S(2)}) copy-start(bf16[512,2048]{1,0:T(8,128)(2,1)} %param.29) | copy-start | bytes 6291460
  11.4 0.7 copy-start.11
  39.7 15.9 %copy-start.10 = (bf16[512,32]{0,1:T(8,128)(2,1)S(1)}, bf16[512,32]{0,1:T(8,128)(2,1)}, u32[]{:S(2)}) copy-start(bf16[512,32]{0,1:T(8,128)(2,1)} %param.21) | copy-start | bytes 98308
  39.7 17.7 %copy-start.5 = (bf16[512,512]{1,0:T(8,128)(2,1)S(1)}, bf16[512,512]{1,0:T(8,128)(2,1)}, u32[]{:S(2)}) copy-start(bf16[512,512]{1,0:T(8,128)(2,1)} %param.20) | copy-start | bytes 1572868
  39.7 17.9 %copy-start.13 = (f32[512]{0:T(512)S(1)}, f32[512]{0:T(512)}, u32[]{:S(2)}) copy-start(f32[512]{0:T(512)} %param.23) | copy-start | bytes 6148
  55.5 145.3 %all-gather.3.cloned.1.call-start = ((), (), s32[]{:S(2)}) async-start(), calls=%async_computation.4 | async-start | bytes 11141120 | tf_op jit(solution)/shard_map/all_gather | solution.py:14
  57.6 2.8 copy-start.15
  57.8 2.3 copy-start.6
  59.7 2.1 copy-start.8
  59.7 2.1 copy-start.9
  59.8 226.9 %reduce-scatter.7.cloned.1.call-start = ((), (), s32[]{:S(2)}) async-start(), calls=%async_computation.7 | async-start | bytes 6684672
  60.0 1.9 copy-start.7
  60.0 1.9 copy-start.14
  183.0 163.8 %reduce-scatter.5.cloned.1.call-start = ((), (), s32[]{:S(2)}) async-start(), calls=%async_computation.5 | async-start | bytes 2228224 | tf_op jit(solution)/shard_map/reduce_scatter | solution.py:136
  200.8 1.6 slice-start
  203.2 7.2 %copy-start.3 = (bf16[512,128]{1,0:T(8,128)(2,1)S(1)}, bf16[512,128]{1,0:T(8,128)(2,1)}, u32[]{:S(2)}) copy-start(bf16[512,128]{1,0:T(8,128)(2,1)} %param.26) | copy-start | bytes 393220
  203.2 7.2 %copy-start.4 = (bf16[512,128]{1,0:T(8,128)(2,1)S(1)}, bf16[512,128]{1,0:T(8,128)(2,1)}, u32[]{:S(2)}) copy-start(bf16[512,128]{1,0:T(8,128)(2,1)} %param.27) | copy-start | bytes 393220
  286.6 9.6 %copy-start.12 = (f32[512,2]{0,1:T(2,128)S(1)}, f32[512,2]{0,1:T(2,128)}, u32[]{:S(2)}) copy-start(f32[512,2]{0,1:T(2,128)} %param.32) | copy-start | bytes 12292
  288.8 58.1 %copy-start.1 = (bf16[2,256,2048]{2,1,0:T(8,128)(2,1)S(1)}, bf16[2,256,2048]{2,1,0:T(8,128)(2,1)}, u32[]{:S(2)}) copy-start(bf16[2,256,2048]{2,1,0:T(8,128)(2,1)} %param.35) | copy-start | bytes 6291460
  290.6 13.0 %all-to-all-start.1 = ((bf16[16,2,48,128]{3,2,1,0:T(8,128)(2,1)}), bf16[16,2,48,128]{3,2,1,0:T(8,128)(2,1)S(1)}, u32[]{:S(2)}, u32[]{:S(2)}) async-start(bf16[16,2,48,128]{3,2,1,0:T(8,128)(2,1)} %copy.48), calls=%async_computation.2 | async-start | bytes 786432 | tf_op jit(solution)/shard_map/all_to_all | solution.py:180
Sparse Core Ops, SparseCore 0:
  55.7 58.0 all-gather.4
  116.2 84.5 all-gather.2
  203.4 66.9 reduce-scatter.6
  286.8 60.0 reduce-scatter.4
where the time goes:
time: 356 us; the launch traced here: 353 us
  waiting for transfers between devices  113 us (32%)
  local copies, waits for them, and re-layouts  88.8 us (25%)
  matrix products  88.1 us (25%)
  other arithmetic  27.5 us (8%)
  blocking collectives  14.7 us (4%)
  between operations  14.3 us (4%)
  starting transfers between devices  6.26 us (2%)
    unnamed x38, local copies, waits for them, and re-layouts  56.3 us
    all_gather x1, waiting for transfers between devices, experts(): piece = lax.all_gather(arrived, 'tp', axis=3, tiled=True)  51.3 us
    reduce_scatter x1, waiting for transfers between devices, token_mixer(): lax.psum_scatter(jnp.dot(attended, output_weight, preferred_element_type=...  36.6 us
    dot_general x16, matrix products, scan_step(): jnp.dot(latent_block, value_weight, preferred_element_type=jnp.float32)  21.8 us
    dot_general x16, matrix products, scan_step(): jnp.dot(latent_block, key_weight, preferred_element_type=jnp.float32)  21.7 us
    all_gather x1, waiting for transfers between devices, sent_together(): out, at, outs = (lax.all_gather(both, axis, axis=dim, tiled=True), 0, [])  17.5 us
    all_to_all x1, blocking collectives, experts(): lax.all_to_all(outgoing, 'ep', split_axis=0, concat_axis=0, tiled=True)  14.7 us
    dot_general x1, matrix products, experts(): jnp.einsum('secf,efd->secd', hidden, down_weight, preferred_element_type=...  10 us
  transfers between devices with their start and end apart: 5, of which 4 were waited for; matrix products, arithmetic and copies ran while one was open for 48% of the time, Pallas kernels for 0%

commit v1 on v0

--- a/solution.py
+++ b/solution.py
@@ -165,7 +165,7 @@
         group_count, local_count, capacity, part_width
     )
     arrived = lax.all_to_all(outgoing, "ep", split_axis=0, concat_axis=0, tiled=True)
-    piece = lax.all_gather(arrived, "tp", axis=3, tiled=True)
+    piece = jnp.concatenate(lax.all_gather(arrived, "tp"), axis=3)
     gate_running = jnp.einsum(
         "secd,edf->secf", piece, gate_weight, preferred_element_type=jnp.float32
     )

time: 356 us -> 349 us (0.980)
  waiting for transfers between devices: 113 us -> 81.6 us
  local copies, waits for them, and re-layouts: 88.8 us -> 111 us
    reshape x0 -> x2, local copies, waits for them, and re-layouts: none -> 23.1 us  [experts(): piece = jnp.concatenate(lax.all_gather(arrived, 'tp'), axis=3)]
    all_gather x1, waiting for transfers between devices: 17.5 us -> 0.02 us  [sent_together(): out, at, outs = (lax.all_gather(both, axis, axis=dim, tiled=True), 0, [])]
    all_gather x1, waiting for transfers between devices: 51.3 us -> 40.4 us  [experts(): piece = jnp.concatenate(lax.all_gather(arrived, 'tp'), axis=3)]
  transfers between devices with their start and end apart: 5 -> 5, of which waited for: 4 -> 3; matrix products, arithmetic and copies ran while one was open for 48% -> 56% of each run, Pallas kernels for 0% -> 0%
where the time goes in v1:
time: 349 us; the launch traced here: 346 us
  local copies, waits for them, and re-layouts  111 us (32%)
  matrix products  88.2 us (25%)
  waiting for transfers between devices  81.6 us (23%)
  other arithmetic  27.5 us (8%)
  blocking collectives  14.8 us (4%)
  between operations  14.3 us (4%)
  starting transfers between devices  7.53 us (2%)
    unnamed x38, local copies, waits for them, and re-layouts  56.3 us
    all_gather x1, waiting for transfers between devices, experts(): piece = jnp.concatenate(lax.all_gather(arrived, 'tp'), axis=3)  40.4 us
    reduce_scatter x1, waiting for transfers between devices, token_mixer(): lax.psum_scatter(jnp.dot(attended, output_weight, preferred_element_type=...  33.4 us
    reshape x2, local copies, waits for them, and re-layouts, experts(): piece = jnp.concatenate(lax.all_gather(arrived, 'tp'), axis=3)  23.1 us
    dot_general x16, matrix products, scan_step(): jnp.dot(latent_block, key_weight, preferred_element_type=jnp.float32)  21.8 us
    dot_general x16, matrix products, scan_step(): jnp.dot(latent_block, value_weight, preferred_element_type=jnp.float32)  21.7 us
    all_to_all x1, blocking collectives, experts(): lax.all_to_all(outgoing, 'ep', split_axis=0, concat_axis=0, tiled=True)  14.8 us
    dot_general x1, matrix products, experts(): jnp.einsum('secf,efd->secd', hidden, down_weight, preferred_element_type=...  10 us
  transfers between devices with their start and end apart: 5, of which 3 were waited for; matrix products, arithmetic and copies ran while one was open for 56% of the time, Pallas kernels for 0%

profile of v1, /device:TPU:6, one launch (start us, length us, event | category | flops | bytes accessed | tf_op | source)
XLA Modules:
  0.0 346.2 jit_solution(7110002154780229827)
XLA Ops:
  7.2 4.2 %convert_element_type.83 = f32[512,2048]{1,0:T(8,128)} convert(bf16[512,2048]{1,0:T(8,128)(2,1)} %param.29) | non-fusion elementwise | flops 1048576 | bytes 6291456 | tf_op jit(solution)/shard_map/convert_element_type | solution.py:22
  12.7 9.0 %reduce-window.6 = s32[32,8,128]{2,1,0:T(8,128)S(1)} reduce-window(s32[32,8,128]{2,1,0:T(8,128)S(1)} %fusion.46, s32[]{:T(128)} %constant.30.clone.1), window={size=1x1x128 pad=0_0x0_0x127_0}, to_apply=%region_8.9 | reduce-window | flops 4161536 | bytes 262148 | tf_op jit(solution)/shard_map/reduce-window
  22.6 4.3 %scatter_custom_fusion = s32[1536]{0:T(1024)S(1)} fusion(s32[1024]{0:T(1024)S(1)} %bitcast.158, s32[1024]{0:T(1024)S(1)} %add_select_fusion, s32[]{:T(128)} %constant.30.clone.1), kind=kCustom, calls=%fused_computation.89 | custom fusion | bytes 6148 | tf_op jit(solution)/shard_map/scatter | solution.py:160
  26.9 7.6 %scatter_custom_fusion.1 = bf16[1536]{0:T(1024)(128)(2,1)S(1)} fusion(s32[1024]{0:T(1024)S(1)} %bitcast.159, bf16[1024]{0:T(1024)(128)(2,1)S(1)} %broadcast.163, bf16[]{:T(256)} %constant.82.clone.1), kind=kCustom, calls=%fused_computation.93 | custom fusion | bytes 3074 | tf_op jit(solution)/shard_map/scatter | solution.py:161
  36.5 3.2 gather_fusion
  40.0 14.8 %all_to_all.10 = bf16[16,2,48,128]{3,2,1,0:T(8,128)(2,1)} all-to-all(bf16[16,2,48,128]{3,2,1,0:T(8,128)(2,1)S(1)} %broadcast_multiply_fusion), channel_id=1, replica_groups=mesh['ep'=16,'tp'=16] {'ep'}, dimensions={0} | all-to-all | bytes 786432 | tf_op jit(solution)/shard_map/all_to_all | solution.py:167
  57.1 1.9 pad_maximum_fusion
  59.7 1.5 fusion.38
  61.8 40.4 %all-gather.6.cloned.1.call-done = bf16[256,2,48,128]{3,2,1,0:T(8,128)(2,1)} async-done(((bf16[16,2,48,128]{3,2,1,0:T(8,128)(2,1)}), bf16[256,2,48,128]{3,2,1,0:T(8,128)(2,1)}) %all-gather.6.cloned.1.call-update) | async-done | bytes 6291472 | tf_op jit(solution)/shard_map/all_gather | solution.py:168
  102.2 12.7 %copy.46 = bf16[16,2,48,16,128]{4,3,2,0,1:T(8,128)(2,1)} copy(bf16[16,2,48,16,128]{4,2,1,0,3:T(8,128)(2,1)} %bitcast.148) | data formatting | bytes 12582912 | tf_op jit(solution)/shard_map/reshape | solution.py:168
  114.9 10.4 %reshape.190 = bf16[16,2,48,2048]{3,2,0,1:T(8,128)(2,1)} reshape(bf16[16,2,48,16,128]{4,3,2,0,1:T(8,128)(2,1)} %copy.46) | data formatting | bytes 12582912 | tf_op jit(solution)/shard_map/reshape | solution.py:168
  125.4 6.5 %fusion.23 = f32[2,16,48,256]{3,2,1,0:T(8,128)} fusion(bf16[16,2,48,2048]{3,2,0,1:T(8,128)(2,1)} %reshape.190, bf16[2,2048,256]{2,1,0:T(8,128)(2,1)} %param.33), kind=kOutput, calls=%fused_computation.40 | convolution fusion | flops 1610612736 | bytes 9961472 | tf_op jit(solution)/shard_map/secd,edf->secf/dot_general | solution.py:169
  131.9 10.0 %convert_bitcast_fusion = bf16[16,2,48,2048]{3,2,0,1:T(8,128)(2,1)} fusion(bf16[2,256,2048]{2,1,0:T(8,128)(2,1)S(1)} %copy-done, f32[2,16,48,256]{3,2,1,0:T(8,128)} %fusion.23, bf16[16,2,48,2048]{3,2,0,1:T(8,128)(2,1)} %reshape.190, bf16[2,2048,256]{2,1,0:T(8,128)(2,1)} %param.34), kind=kOutput, calls=%fused_computation.29 | convolution fusion | flops 3226730496 | bytes 18350080 | tf_op jit(solution)/shard_map/secf,efd->secd/dot_general | solution.py:174
  141.9 23.1 %copy.55 = bf16[16,2,48,2048]{2,0,1,3:T(8,128)(2,1)} copy(bf16[16,2,48,2048]{3,2,0,1:T(8,128)(2,1)} %convert_bitcast_fusion) | data formatting | bytes 12582912
  164.9 29.7 %reshape.233 = bf16[2048,1536]{1,0:T(8,128)(2,1)} reshape(bf16[2048,2,16,48]{3,2,1,0:T(8,128)(2,1)} %bitcast.142) | data formatting | bytes 12582912
  194.7 1.6 slice-done
  197.2 7.2 %slice.38 = bf16[8192,512]{1,0:T(8,128)(2,1)} slice(bf16[8192,544]{1,0:T(8,128)(2,1)} %all-gather.4.cloned.1.call-done), slice={[0:8192], [0:512]} | slice | bytes 16777216 | tf_op jit(solution)/shard_map/slice | solution.py:16
  204.3 73.1 %while.15 = (s32[]{:T(128)}, f32[512,2]{0,1:T(2,128)S(1)}, f32[512,2]{0,1:T(2,128)S(1)}, f32[512,2,64]{0,2,1:T(8,128)S(1)}, bf16[16,512,512]{2,1,0:T(8,128)(2,1)...) while((s32[]{:T(128)}, f32[512,2]{0,1:T(2,128)S(1)}, ...), condition=%wide.region_5.6_spmd.clone, body=%wide.region_2.5_spmd.clone.sunk | while | flops 305992704 | bytes 13141125 | solution.py:122
  204.3 1.4 convolution_convert_fusion.6
  211.6 1.4 convolution_convert_fusion.7
  227.2 1.4 convolution_convert_fusion.6
  239.0 1.4 convolution_convert_fusion.7
  245.5 1.4 convolution_convert_fusion.6
  248.2 1.4 convolution_convert_fusion.7
  277.4 3.1 convolution_convert_fusion.2
  280.6 2.1 reshape.234
  282.7 1.8 copy.47
  284.5 7.2 %all-to-all-start.1 = ((bf16[16,2,48,128]{3,2,1,0:T(8,128)(2,1)}), bf16[16,2,48,128]{3,2,1,0:T(8,128)(2,1)S(1)}, u32[]{:S(2)}, u32[]{:S(2)}) async-start(bf16[16,2,48,128]{3,2,1,0:T(8,128)(2,1)} %copy.47), calls=%async_computation.2 | async-start | bytes 786432 | tf_op jit(solution)/shard_map/all_to_all | solution.py:180
  291.9 7.7 %all-to-all-done.1 = bf16[16,2,48,128]{3,2,1,0:T(8,128)(2,1)S(1)} async-done(((bf16[16,2,48,128]{3,2,1,0:T(8,128)(2,1)}), bf16[16,2,48,128]{3,2,1,0:T(8,128)(2,1)S(1)}, u32[]{:S(2)}, u32[]{:S(2)}) %all-to-all-start.1) | async-done | bytes 393248 | tf_op jit(solution)/shard_map/all_to_all | solution.py:180
  299.6 3.2 gather_fusion.1
  302.8 3.5 fusion.37
  306.2 33.4 %reduce-scatter.5.cloned.1.call-done = bf16[32,2048]{1,0:T(8,128)(2,1)} async-done(((bf16[512,2048]{1,0:T(8,128)(2,1)}), bf16[32,2048]{1,0:T(8,128)(2,1)}) %reduce-scatter.5.cloned.1.call-update) | async-done | bytes 131088 | tf_op jit(solution)/shard_map/reduce_scatter | solution.py:136
  (227 shorter events, 72.4 us)
Async XLA Ops:
  7.2 124.7 %copy-start = (bf16[2,256,2048]{2,1,0:T(8,128)(2,1)S(1)}, bf16[2,256,2048]{2,1,0:T(8,128)(2,1)}, u32[]{:S(2)}) copy-start(bf16[2,256,2048]{2,1,0:T(8,128)(2,1)} %param.35) | copy-start | bytes 6291460
  7.2 95.0 %all-gather.6.cloned.1.call-start = ((), (), s32[]{:S(2)}) async-start(), calls=%async_computation.6 | async-start | bytes 6684672 | tf_op jit(solution)/shard_map/all_gather | solution.py:168
  7.2 4.2 %copy-start.2 = (bf16[512,2048]{1,0:T(8,128)(2,1)S(1)}, bf16[512,2048]{1,0:T(8,128)(2,1)}, u32[]{:S(2)}) copy-start(bf16[512,2048]{1,0:T(8,128)(2,1)} %param.29) | copy-start | bytes 6291460
  11.4 0.7 copy-start.11
  36.5 18.4 %copy-start.10 = (bf16[512,32]{0,1:T(8,128)(2,1)S(1)}, bf16[512,32]{0,1:T(8,128)(2,1)}, u32[]{:S(2)}) copy-start(bf16[512,32]{0,1:T(8,128)(2,1)} %param.21) | copy-start | bytes 98308
  39.7 17.0 %copy-start.5 = (bf16[512,512]{1,0:T(8,128)(2,1)S(1)}, bf16[512,512]{1,0:T(8,128)(2,1)}, u32[]{:S(2)}) copy-start(bf16[512,512]{1,0:T(8,128)(2,1)} %param.20) | copy-start | bytes 1572868
  39.7 17.2 %copy-start.13 = (f32[512]{0:T(512)S(1)}, f32[512]{0:T(512)}, u32[]{:S(2)}) copy-start(f32[512]{0:T(512)} %param.23) | copy-start | bytes 6148
  54.8 139.9 %all-gather.4.cloned.1.call-start = ((), (), s32[]{:S(2)}) async-start(), calls=%async_computation.4 | async-start | bytes 11141120 | tf_op jit(solution)/shard_map/all_gather | solution.py:14
  56.9 2.8 copy-start.15
  57.1 2.2 copy-start.6
  59.0 2.1 copy-start.8
  59.0 2.1 copy-start.9
  59.1 221.5 %reduce-scatter.7.cloned.1.call-start = ((), (), s32[]{:S(2)}) async-start(), calls=%async_computation.7 | async-start | bytes 6684672
  59.3 1.9 copy-start.7
  59.3 1.9 copy-start.14
  194.7 145.0 %reduce-scatter.5.cloned.1.call-start = ((), (), s32[]{:S(2)}) async-start(), calls=%async_computation.5 | async-start | bytes 2228224 | tf_op jit(solution)/shard_map/reduce_scatter | solution.py:136
  194.7 1.6 slice-start
  197.1 7.2 %copy-start.3 = (bf16[512,128]{1,0:T(8,128)(2,1)S(1)}, bf16[512,128]{1,0:T(8,128)(2,1)}, u32[]{:S(2)}) copy-start(bf16[512,128]{1,0:T(8,128)(2,1)} %param.26) | copy-start | bytes 393220
  197.1 7.2 %copy-start.4 = (bf16[512,128]{1,0:T(8,128)(2,1)S(1)}, bf16[512,128]{1,0:T(8,128)(2,1)}, u32[]{:S(2)}) copy-start(bf16[512,128]{1,0:T(8,128)(2,1)} %param.27) | copy-start | bytes 393220
  280.6 11.1 %copy-start.12 = (f32[512,2]{0,1:T(2,128)S(1)}, f32[512,2]{0,1:T(2,128)}, u32[]{:S(2)}) copy-start(f32[512,2]{0,1:T(2,128)} %param.32) | copy-start | bytes 12292
  282.7 56.9 %copy-start.1 = (bf16[2,256,2048]{2,1,0:T(8,128)(2,1)S(1)}, bf16[2,256,2048]{2,1,0:T(8,128)(2,1)}, u32[]{:S(2)}) copy-start(bf16[2,256,2048]{2,1,0:T(8,128)(2,1)} %param.35) | copy-start | bytes 6291460
  284.5 15.0 %all-to-all-start.1 = ((bf16[16,2,48,128]{3,2,1,0:T(8,128)(2,1)}), bf16[16,2,48,128]{3,2,1,0:T(8,128)(2,1)S(1)}, u32[]{:S(2)}, u32[]{:S(2)}) async-start(bf16[16,2,48,128]{3,2,1,0:T(8,128)(2,1)} %copy.47), calls=%async_computation.2 | async-start | bytes 786432 | tf_op jit(solution)/shard_map/all_to_all | solution.py:180
Sparse Core Ops, SparseCore 0:
  55.0 47.2 all-gather.5
  104.6 84.0 all-gather.3
  194.8 65.9 reduce-scatter.6
  280.7 58.9 reduce-scatter.4
